TPU v7x, 256 devices: a whole 4x4x8 slice. The times are simulated.
256 devices in a mesh: ep: 32 (over z, x), tp: 8 (over y, core).
Axes of the slice: x: 4, y: 4, z: 8, core: 2. Of those that a mesh axis runs over, the one named last changes fastest.
Arguments:
- tokens: bfloat16 [16384, 4096], P('ep', 'tp'), may hold values from -60 to 60
- routes: int32 [16384, 4], P('ep'), may hold values from 0 to 127, all different within a row; in each aligned block of 512 rows (0 to 511, 512 to 1023, ...) at most 32 rows name the same one
- route_weights: float32 [16384, 4], P('ep'), may hold values from 0.1 to 1
- pre_gain: float32 [4096], P('tp'), may hold values from 0.1 to 1.9
- expert_gate: bfloat16 [128, 4096, 512], P('ep', 'tp'), may hold values from -0.09375 to 0.09375
- expert_up: bfloat16 [128, 4096, 512], P('ep', 'tp'), may hold values from -0.09375 to 0.09375
- expert_down: bfloat16 [128, 512, 4096], P('ep', None, 'tp'), may hold values from -1 to 1
- shared_gate: bfloat16 [4096, 512], P('tp'), may hold values from -0.09375 to 0.09375
- shared_up: bfloat16 [4096, 512], P('tp'), may hold values from -0.09375 to 0.09375
- shared_down: bfloat16 [512, 4096], P(None, 'tp'), may hold values from -1 to 1
- post_gain: float32 [4096], P('tp'), may hold values from 0.1 to 1.9
Outputs:
- layer_out: bfloat16 [16384, 4096], P('ep', 'tp')
Inputs may be any that keep to these rules, and one draw needn't show every extreme that they name: `routes`: each row names 4 different experts. Within each aligned block of 512 rows (the tokens of one index of ep) no expert is named more than 32 times, a bound that some block reaches.
All inputs are finite; a program needn't handle non-finite values.
Results may differ from a plain program's by a relative error of at most 0.022.
Values may be sent and summed in bfloat16 or wider, within the bound.
A program may use at most 128 MiB of HBM per device.

v0:
```python
import jax
import jax.numpy as jnp
from jax import lax
from jax.sharding import PartitionSpec as P

epsilon = 1e-06


def from_everyone(array, axis):
    peers = lax.axis_size(axis)
    return lax.all_to_all(
        jnp.broadcast_to(array[None], (peers, *array.shape)), axis, 0, 0, tiled=True
    )


def of_everyone(array, axis):
    everything = from_everyone(array, axis)
    return jnp.sum(everything, axis=0)


def sent_together(arrays, axis, dim, along):
    both = jnp.concatenate(arrays, axis=along)
    filled, at, outs = (lax.psum_scatter(both, axis, scatter_dimension=dim, tiled=True), 0, [])
    for a in arrays:
        outs.append(lax.slice_in_dim(filled, at, at + a.shape[along], axis=along))
        at += a.shape[along]
    return tuple(outs)


def inverse_norm(values, features):
    squares = jnp.sum(values * values, axis=1)
    totals = of_everyone(squares, "tp")
    return lax.rsqrt(totals / features + epsilon)


def activate(gate_part, up_part):
    gate_pre, up_pre = tuple(
        (
            part.astype(jnp.float32)
            for part in sent_together(
                (gate_part.astype(jnp.bfloat16), up_part.astype(jnp.bfloat16)), "tp", 1, 0
            )
        )
    )
    hidden_share = (jax.nn.silu(gate_pre) * up_pre).astype(jnp.bfloat16)
    return lax.all_gather(hidden_share, "tp", axis=1, tiled=True)


def per_device(
    tokens,
    routes,
    route_weights,
    pre_gain,
    expert_gate,
    expert_up,
    expert_down,
    shared_gate,
    shared_up,
    shared_down,
    post_gain,
):
    slice_width = tokens.shape[1]
    features = slice_width * lax.axis_size("tp")
    groups = lax.axis_size("ep")
    local_experts = expert_gate.shape[0]
    token_count, fanout = routes.shape
    capacity = 2 * token_count * fanout // (local_experts * groups)
    rows_all = local_experts * groups * capacity
    inputs = tokens.astype(jnp.float32)
    normed = (inputs * inverse_norm(inputs, features)[:, None] * pre_gain).astype(jnp.bfloat16)
    flat_ids = routes.reshape(-1)
    one_hot = (
        flat_ids[:, None] == jnp.arange(local_experts * groups, dtype=jnp.int32)[None, :]
    ).astype(jnp.int32)
    slots = jnp.sum(jnp.cumsum(one_hot, axis=0) * one_hot, axis=1) - 1
    positions = flat_ids * capacity + slots
    token_index = jnp.arange(flat_ids.shape[0], dtype=jnp.int32) // fanout
    outgoing = (
        jnp.zeros((rows_all, slice_width), jnp.bfloat16).at[positions].set(normed[token_index])
    )
    outgoing = outgoing.reshape(groups, local_experts, capacity, slice_width)
    arrived = lax.all_to_all(outgoing, "ep", split_axis=0, concat_axis=2, tiled=True)[0]
    gate_part = jnp.einsum("erd,edf->erf", arrived, expert_gate, preferred_element_type=jnp.float32)
    up_part = jnp.einsum("erd,edf->erf", arrived, expert_up, preferred_element_type=jnp.float32)
    hidden = activate(gate_part.reshape(rows_all, -1), up_part.reshape(rows_all, -1))
    hidden = hidden.reshape(local_experts, groups * capacity, -1)
    expert_out = jnp.einsum(
        "erf,efd->erd", hidden, expert_down, preferred_element_type=jnp.float32
    ).astype(jnp.bfloat16)
    returned = lax.all_to_all(expert_out[None], "ep", split_axis=2, concat_axis=0, tiled=True)
    copies = returned.reshape(rows_all, slice_width)[positions].astype(jnp.float32)
    routed = jnp.sum(
        copies.reshape(token_count, fanout, slice_width) * route_weights[:, :, None], axis=1
    )
    shared_gate_part = jnp.dot(normed, shared_gate, preferred_element_type=jnp.float32)
    shared_up_part = jnp.dot(normed, shared_up, preferred_element_type=jnp.float32)
    shared_hidden = activate(shared_gate_part, shared_up_part)
    shared_out = jnp.dot(shared_hidden, shared_down, preferred_element_type=jnp.float32).astype(
        jnp.bfloat16
    )
    mixture = routed + shared_out.astype(jnp.float32)
    return (mixture * inverse_norm(mixture, features)[:, None] * post_gain).astype(jnp.bfloat16)


def solution(mesh):
    in_specs = (
        P("ep", "tp"),
        P("ep", None),
        P("ep", None),
        P("tp"),
        P("ep", "tp", None),
        P("ep", "tp", None),
        P("ep", None, "tp"),
        P("tp", None),
        P("tp", None),
        P(None, "tp"),
        P("tp"),
    )
    out_specs = P("ep", "tp")
    return jax.shard_map(
        per_device, mesh=mesh, in_specs=in_specs, out_specs=out_specs, check_vma=False
    )
```

profile of v0, /device:TPU:1, one launch (start us, length us, event | category | flops | bytes accessed | tf_op | source)
XLA Modules:
  0.0 432.0 jit_solution(670776290911037855)
XLA Ops:
  6.5 0.0 copy-start
  6.5 1.4 fusion.5
  7.9 0.6 broadcast_in_dim.9
  8.5 6.4 %all-to-all-start = ((f32[8,1,512]{2,1,0:T(1,128)}), f32[8,1,512]{2,1,0:T(1,128)S(1)}, u32[]{:S(2)}, u32[]{:S(2)}) async-start(f32[8,1,512]{2,1,0:T(1,128)} %broadcast_in_dim.9), calls=%async_computation | async-start | bytes 32768 | tf_op jit(solution)/shard_map/all_to_all | solution.py:11
  15.0 0.0 reduce-scatter.7.cloned.1.call-start
  15.0 0.8 copy.69
  15.8 0.2 eq.29
  16.0 0.2 eq.25
  16.2 0.7 broadcast_multiply_fusion
  16.9 0.1 copy.71
  17.0 0.3 fusion.13
  17.4 0.1 broadcast_add_fusion
  17.4 0.3 copy.72
  17.8 0.6 fusion.12
  18.4 0.1 copy.68
  18.6 0.2 mul.81
  18.8 0.8 all-to-all-done
  19.7 0.0 copy-done.5
  19.7 1.2 fusion.7
  20.9 21.3 %scatter_custom_fusion = bf16[4096,512]{1,0:T(8,128)(2,1)} fusion(s32[2048]{0:T(1024)S(1)} %bitcast.53, bf16[512,512]{1,0:T(8,128)(2,1)S(1)} %fusion.7, s32[2048]{0:T(1024)S(1)} %broadcast_clamp_fusion.1, bf16[]{:T(256)} %constant.34.clone.1), kind=kCustom, calls=%fused_computation.8 | custom fusion | bytes 4194306 | tf_op jit(solution)/shard_map/scatter | solution.py:79
  42.2 104.1 %all_to_all.42 = bf16[32,4,32,512]{3,2,1,0:T(8,128)(2,1)S(1)} all-to-all(bf16[32,4,32,512]{3,2,1,0:T(8,128)(2,1)} %bitcast.43), channel_id=1, replica_groups=mesh['ep'=32,'tp'=8] {'ep'}, dimensions={0} | all-to-all | bytes 8388608 | tf_op jit(solution)/shard_map/all_to_all | solution.py:82
  146.3 0.6 copy.74
  146.9 0.0 copy-done
  146.9 0.0 copy-start.7
  146.9 4.3 convolution_convert_fusion.1
  151.2 0.0 copy-done.7
  151.2 4.3 convolution_convert_fusion
  155.6 7.2 %pad_maximum_fusion = bf16[8192,512]{1,0:T(8,128)(2,1)} fusion(bf16[4096,512]{1,0:T(8,128)(2,1)} %bitcast.50, bf16[4096,512]{1,0:T(8,128)(2,1)} %bitcast.49), kind=kLoop, calls=%fused_computation.3 | loop fusion | flops 16777216 | bytes 16777216 | tf_op jit(solution)/shard_map/concatenate | solution.py:22
  162.8 11.4 %copy.86 = bf16[8192,512]{0,1:T(8,128)(2,1)} copy(bf16[8192,512]{1,0:T(8,128)(2,1)} %pad_maximum_fusion) | data formatting | bytes 16777216
  174.1 0.0 reduce-scatter.7.cloned.1.call-update
  174.2 0.0 all-gather.2.cloned.1.call-start
  174.2 53.1 %reduce-scatter.7.cloned.1.call-done = bf16[64,8192]{1,0:T(8,128)(2,1)} async-done(((bf16[512,8192]{1,0:T(8,128)(2,1)}), bf16[64,8192]{1,0:T(8,128)(2,1)}) %reduce-scatter.7.cloned.1.call-update) | async-done | bytes 1048592
  227.3 2.3 fusion.15
  229.6 0.0 all-gather.2.cloned.1.call-update
  229.6 0.0 copy-start.8
  229.6 35.3 %all-gather.2.cloned.1.call-done = bf16[4096,512]{0,1:T(8,128)(2,1)} async-done(((bf16[4096,64]{0,1:T(8,128)(2,1)}), bf16[4096,512]{0,1:T(8,128)(2,1)}) %all-gather.2.cloned.1.call-update) | async-done | bytes 4194320 | tf_op jit(solution)/shard_map/all_gather | solution.py:46
  265.0 6.5 %copy.77 = bf16[4096,512]{1,0:T(8,128)(2,1)} copy(bf16[4096,512]{0,1:T(8,128)(2,1)} %all-gather.2.cloned.1.call-done) | data formatting | bytes 8388608 | tf_op jit(solution)/shard_map/all_gather | solution.py:46
  271.5 0.0 copy-done.8
  271.5 4.5 %convert_bitcast_fusion = bf16[1,4,1024,512]{3,2,1,0:T(8,128)(2,1)S(1)} fusion(bf16[4,1024,512]{2,1,0:T(8,128)(2,1)} %bitcast.47, bf16[4,512,512]{2,1,0:T(8,128)(2,1)S(1)} %copy-done.8), kind=kOutput, calls=%fused_computation.5 | convolution fusion | flops 2149580800 | bytes 10485760 | tf_op jit(solution)/shard_map/erf,efd->erd/dot_general | solution.py:87
  276.1 5.2 %copy.78 = bf16[1,4,1024,512]{3,1,0,2:T(4,128)(2,1)} copy(bf16[1,4,1024,512]{3,2,1,0:T(8,128)(2,1)S(1)} %convert_bitcast_fusion) | data formatting | bytes 8388608 | tf_op jit(solution)/shard_map/broadcast_in_dim | solution.py:90
  281.3 9.8 %all-to-all-start.2 = ((bf16[1,4,1024,512]{3,1,0,2:T(4,128)(2,1)}), bf16[1,4,1024,512]{3,1,0,2:T(4,128)(2,1)}, u32[]{:S(2)}, u32[]{:S(2)}) async-start(bf16[1,4,1024,512]{3,1,0,2:T(4,128)(2,1)} %copy.78), calls=%async_computation.2 | async-start | bytes 8388608 | tf_op jit(solution)/shard_map/all_to_all | solution.py:90
  291.1 0.0 copy-start.4
  291.1 0.0 reduce-scatter.9.cloned.1.call-start
  291.1 0.0 copy-done.2
  291.1 0.4 convolution_convert_fusion.3
  291.6 0.4 convolution_convert_fusion.4
  292.0 0.1 pad_maximum_fusion.1
  292.1 1.4 copy.88
  293.5 0.0 reduce-scatter.9.cloned.1.call-update
  293.5 0.0 copy-done.4
  293.5 0.1 copy.80
  293.7 33.9 %reduce-scatter.9.cloned.1.call-done = bf16[64,1024]{1,0:T(8,128)(2,1)} async-done(((bf16[512,1024]{1,0:T(8,128)(2,1)}), bf16[64,1024]{1,0:T(8,128)(2,1)}) %reduce-scatter.9.cloned.1.call-update) | async-done | bytes 131088
  327.6 0.9 fusion.21
  328.5 17.2 %all_gather.7 = bf16[512,512]{0,1:T(8,128)(2,1)} all-gather(bf16[512,64]{0,1:T(8,128)(2,1)S(1)} %fusion.21), channel_id=1, replica_groups=mesh['ep'=32,'tp'=8] {'tp'}, dimensions={1}, use_global_device_ids=true | all-gather | bytes 589824 | tf_op jit(solution)/shard_map/all_gather | solution.py:46
  345.7 38.9 %all-to-all-done.2 = bf16[1,4,1024,512]{3,1,0,2:T(4,128)(2,1)} async-done(((bf16[1,4,1024,512]{3,1,0,2:T(4,128)(2,1)}), bf16[1,4,1024,512]{3,1,0,2:T(4,128)(2,1)}, u32[]{:S(2)}, u32[]{:S(2)}) %all-to-all-start.2) | async-done | bytes 4194336 | tf_op jit(solution)/shard_map/all_to_all | solution.py:90
  384.6 5.5 %copy.79 = bf16[1,4,32,32,512]{4,3,1,2,0:T(8,128)(2,1)} copy(bf16[1,4,32,32,512]{4,1,3,2,0:T(4,128)(2,1)} %bitcast.14) | data formatting | bytes 8388608 | tf_op jit(solution)/shard_map/all_to_all | solution.py:90
  390.1 10.3 %gather_fusion = bf16[2048,512]{1,0:T(8,128)(2,1)S(1)} fusion(bf16[4096,512]{1,0:T(8,128)(2,1)} %bitcast.41, s32[2048]{0:T(1024)S(1)} %broadcast_clamp_fusion), kind=kCustom, calls=%fused_computation.1 | custom fusion | bytes 4202496 | tf_op jit(solution)/shard_map/gather | solution.py:91
  400.4 3.0 reshape.142
  403.5 4.9 %multiply_reduce_fusion = f32[512,512]{1,0:T(8,128)S(1)} fusion(f32[512,4,512]{2,1,0:T(4,128)} %reshape.142, f32[512,4]{1,0:T(8,128)S(1)} %copy.80), kind=kLoop, calls=%fused_computation.4 | loop fusion | flops 1835008 | bytes 5251072 | tf_op jit(solution)/shard_map/reduce_sum | solution.py:92
  408.4 1.3 copy.83
  409.7 2.0 multiply_reduce_fusion.1
  411.8 10.7 %all_to_all.43 = f32[8,1,512]{2,1,0:T(1,128)S(1)} all-to-all(f32[8,1,512]{2,1,0:T(1,128)S(1)} %broadcast_in_dim.11), channel_id=1, replica_groups=mesh['ep'=32,'tp'=8] {'tp'}, dimensions={0} | all-to-all | bytes 32768 | tf_op jit(solution)/shard_map/all_to_all | solution.py:11
  422.5 0.9 multiply_convert_fusion
  423.5 2.0 copy.85
  (21 shorter events, 0.2 us)
Async XLA Ops:
  6.5 140.4 %copy-start = (bf16[4,512,512]{2,1,0:T(8,128)(2,1)S(1)}, bf16[4,512,512]{2,1,0:T(8,128)(2,1)}, u32[]{:S(2)}) copy-start(bf16[4,512,512]{2,1,0:T(8,128)(2,1)} %param.15) | copy-start | bytes 6291460
  6.5 13.2 %copy-start.5 = (f32[512]{0:T(512)S(1)}, f32[512]{0:T(512)}, u32[]{:S(2)}) copy-start(f32[512]{0:T(512)} %param.14) | copy-start | bytes 6148
  8.5 11.1 %all-to-all-start = ((f32[8,1,512]{2,1,0:T(1,128)}), f32[8,1,512]{2,1,0:T(1,128)S(1)}, u32[]{:S(2)}, u32[]{:S(2)}) async-start(f32[8,1,512]{2,1,0:T(1,128)} %broadcast_in_dim.9), calls=%async_computation | async-start | bytes 32768 | tf_op jit(solution)/shard_map/all_to_all | solution.py:11
  15.0 212.3 %reduce-scatter.7.cloned.1.call-start = ((), (), s32[]{:S(2)}) async-start(), calls=%async_computation.7 | async-start | bytes 9437184
  146.9 4.3 copy-start.7
  174.2 90.8 %all-gather.2.cloned.1.call-start = ((), (), s32[]{:S(2)}) async-start(), calls=%async_computation.6 | async-start | bytes 4718592 | tf_op jit(solution)/shard_map/all_gather | solution.py:46
  229.6 41.9 %copy-start.8 = (bf16[4,512,512]{2,1,0:T(8,128)(2,1)S(1)}, bf16[4,512,512]{2,1,0:T(8,128)(2,1)}, u32[]{:S(2)}) copy-start(bf16[4,512,512]{2,1,0:T(8,128)(2,1)} %param.17) | copy-start | bytes 6291460
  281.3 9.9 %copy-start.2 = (bf16[512,512]{1,0:T(8,128)(2,1)S(1)}, bf16[512,512]{1,0:T(8,128)(2,1)}, u32[]{:S(2)}) copy-start(bf16[512,512]{1,0:T(8,128)(2,1)} %param.19) | copy-start | bytes 1572868
  281.3 10.3 %copy-start.3 = (bf16[512,512]{1,0:T(8,128)(2,1)S(1)}, bf16[512,512]{1,0:T(8,128)(2,1)}, u32[]{:S(2)}) copy-start(bf16[512,512]{1,0:T(8,128)(2,1)} %param.18) | copy-start | bytes 1572868
  281.3 103.3 %all-to-all-start.2 = ((bf16[1,4,1024,512]{3,1,0,2:T(4,128)(2,1)}), bf16[1,4,1024,512]{3,1,0,2:T(4,128)(2,1)}, u32[]{:S(2)}, u32[]{:S(2)}) async-start(bf16[1,4,1024,512]{3,1,0,2:T(4,128)(2,1)} %copy.78), calls=%async_computation.2 | async-start | bytes 8388608 | tf_op jit(solution)/shard_map/all_to_all | solution.py:90
  291.1 2.5 copy-start.4
  291.1 36.5 %reduce-scatter.9.cloned.1.call-start = ((), (), s32[]{:S(2)}) async-start(), calls=%async_computation.8 | async-start | bytes 1179648
  403.5 19.1 %copy-start.6 = (f32[512]{0:T(512)S(1)}, f32[512]{0:T(512)}, u32[]{:S(2)}) copy-start(f32[512]{0:T(512)} %param.21) | copy-start | bytes 6148
  403.5 22.0 %copy-start.1 = (bf16[4,512,512]{2,1,0:T(8,128)(2,1)S(1)}, bf16[4,512,512]{2,1,0:T(8,128)(2,1)}, u32[]{:S(2)}) copy-start(bf16[4,512,512]{2,1,0:T(8,128)(2,1)} %param.15) | copy-start | bytes 6291460
Sparse Core Ops, SparseCore 0:
  174.3 52.9 reduce-scatter.6
  229.8 35.1 all-gather.1
  294.4 33.0 reduce-scatter.8
where the time goes:
time: 434 us; the launch traced here: 432 us
  waiting for transfers between devices  162 us (37%)
  blocking collectives  132 us (30%)
  local copies, waits for them, and re-layouts  71.3 us (16%)
  other arithmetic  20.9 us (5%)
  starting transfers between devices  16.3 us (4%)
  matrix products  16 us (4%)
  between operations  13.4 us (3%)
    all_to_all x1, blocking collectives, per_device(): lax.all_to_all(outgoing, 'ep', split_axis=0, concat_axis=2, tiled=True)[0]  104 us
    unnamed x5, waiting for transfers between devices  87 us
    all_to_all x1, waiting for transfers between devices, per_device(): lax.all_to_all(expert_out[None], 'ep', split_axis=2, concat_axis=0, tiled...  38.9 us
    all_gather x1, waiting for transfers between devices, activate(): return lax.all_gather(hidden_share, 'tp', axis=1, tiled=True)  35.3 us
    scatter x1, local copies, waits for them, and re-layouts, per_device(): jnp.zeros((rows_all, slice_width), jnp.bfloat16).at[positions]  21.3 us
    all_gather x1, blocking collectives, activate(): return lax.all_gather(hidden_share, 'tp', axis=1, tiled=True)  17.2 us
    unnamed x22, local copies, waits for them, and re-layouts  13.8 us
    all_to_all x1, blocking collectives, from_everyone(): lax.all_to_all(jnp.broadcast_to(array[None], (peers, *array.shape)), axis...  10.7 us
  transfers between devices with their start and end apart: 5, of which 5 were waited for; matrix products, arithmetic and copies ran while one was open for 2% of the time, Pallas kernels for 0%

commit v1 on v0

v1 whole, which is shorter than its diff:
```python
import functools

import jax
import jax.numpy as jnp
from jax import lax
from jax.experimental import pallas as pl
from jax.experimental.pallas import tpu as pltpu
from jax.sharding import PartitionSpec as P

MESH = pl.DeviceIdType.MESH
BF, F32 = jnp.bfloat16, jnp.float32
epsilon = 1e-06

NX, NC = 4, 2
CAP = 32

STAGES = ((0,), (1, 7), (2, 6), (3, 5), (4,), None)
SHARED = 5
OFFSET = (0, 64, 192, 320, 448, 512)
ROWS = 576

SCHEDULE = " ".join(
    (
        "A0 B0 C5 D5",
        "A1 B1 E5 C0",
        "D0 F5 A2 B2",
        "E0 C1 D1 A3",
        "B3 F0 G5 G0",
        "E1 C2 D2 A4",
        "B4 F1 G1 E2",
        "C4 D4 F2 C3",
        "D3 G2 E4 F4",
        "G4 E3 F3 G3",
        "Z4 Z3 Z2 Z1",
        "Z0",
    )
).split()


def kernel(
    nz,
    ny,
    features,
    schedule,
    tok_hbm,
    meta_in,
    gain,
    post,
    wg_hbm,
    wu_hbm,
    wd_hbm,
    sg_hbm,
    su_hbm,
    sd_hbm,
    out_ref,
    normed,
    wg,
    wu,
    wd,
    blocks,
    meta,
    inv,
    rows_out,
    rows_in,
    own_part,
    for_partner,
    from_partner,
    from_y,
    hid,
    returned,
    shared_out,
    z_in,
    part,
    mix,
    sums,
    send_sem,
    recv_sem,
    local_sem,
):
    ep, tp = lax.axis_index("ep"), lax.axis_index("tp")
    z, x = ep // NX, ep % NX
    y, c = tp // NC, tp % NC
    n_tok = normed.shape[0]
    half = n_tok // 2

    def device(dz=0, dx=0, dy=0, dc=0):
        return (
            (z + dz + nz) % nz * NX + (x + dx + NX) % NX,
            (y + dy + ny) % ny * NC + (c + dc) % NC,
        )

    used = [0, 0]
    sends, awaited = {}, {}

    def push(src, dst, to):
        i = used[0]
        used[0] += 1
        copy = pltpu.make_async_remote_copy(
            src_ref=src,
            dst_ref=dst,
            send_sem=send_sem.at[i],
            recv_sem=recv_sem.at[i],
            device_id=to,
            device_id_type=MESH,
        )
        copy.start()
        sends[id(copy)] = copy
        awaited[id(copy)] = copy
        return copy

    def got(copy):
        awaited.pop(id(copy)).wait_recv()

    def sent(copies):
        for copy in copies:
            sends.pop(id(copy)).wait_send()

    def load(src, dst):
        copy = pltpu.make_async_copy(src, dst, local_sem.at[used[1]])
        used[1] += 1
        copy.start()
        return copy

    token_load = load(tok_hbm, blocks.at[0])
    weight_loads = {
        "shared": [load(sg_hbm, wg.at[4]), load(su_hbm, wu.at[4])],
        "up": [load(wg_hbm, wg.at[pl.ds(0, 4)]), load(wu_hbm, wu.at[pl.ds(0, 4)])],
        "down": [load(sd_hbm, wd.at[4]), load(wd_hbm, wd.at[pl.ds(0, 4)])],
    }

    def need(name):
        for copy in weight_loads.pop(name, []):
            copy.wait()

    peers = [device(dz=1), device(dz=-1)]
    peers += [device(dx=dx) for dx in range(1, NX)]
    tp_steps = [(dy, dc) for dy in range(ny) for dc in range(NC)][1:]
    peers += [device(dy=dy, dc=dc) for dy, dc in tp_steps]
    barrier = pltpu.get_barrier_semaphore()
    for peer in peers:
        pl.semaphore_signal(barrier, inc=1, device_id=peer, device_id_type=MESH)

    def to_row(column):
        n = column.shape[0]
        same = lax.broadcasted_iota(jnp.int32, (n, n), 0) == lax.broadcasted_iota(
            jnp.int32, (n, n), 1
        )
        return jnp.sum(jnp.where(same, column, 0.0), axis=0, keepdims=True)

    def spread(row, width):
        high = row.astype(BF)
        rest = row - high.astype(F32)
        middle = rest.astype(BF)
        low = (rest - middle.astype(F32)).astype(BF)
        left = jnp.concatenate([high, middle, low, jnp.zeros((13, row.shape[1]), BF)], axis=0)
        column = lax.dot_general(
            left, jnp.ones((16, 128), BF), (((0,), (0,)), ((), ())), preferred_element_type=F32
        )
        return jnp.concatenate([column] * (width // 128), axis=1)

    def start_norm(values, which, cols):
        sums[which, 0, :, cols] = to_row(jnp.sum(values * values, axis=1, keepdims=True))
        return [
            push(
                sums.at[which, 0, :, cols],
                sums.at[which, i + 1, :, cols],
                device(dy=dy, dc=dc),
            )
            for i, (dy, dc) in enumerate(tp_steps)
        ]

    def end_norm(copies, which, cols):
        total = sums[which, 0, :, cols]
        for i, copy in enumerate(copies):
            got(copy)
            total = total + sums[which, i + 1, :, cols]
        return lax.rsqrt(total / features + epsilon)

    def place():
        experts = 128
        e_id = lax.broadcasted_iota(jnp.int32, (experts, n_tok), 0).astype(F32)
        named = jnp.zeros((experts, n_tok), F32)
        for k in range(4):
            named += (e_id == meta_in[k : k + 1]).astype(F32)
        before = (
            lax.broadcasted_iota(jnp.int32, (n_tok, n_tok), 0)
            < lax.broadcasted_iota(jnp.int32, (n_tok, n_tok), 1)
        )
        counts = jnp.dot(
            named.astype(BF), before.astype(F32).astype(BF), preferred_element_type=F32
        )
        for k in range(4):
            route = meta_in[k : k + 1]
            slot = jnp.sum(jnp.where(e_id == route, counts, 0.0), axis=0, keepdims=True)
            meta[0, k : k + 1] = route * CAP + slot
        meta[0, 4:8] = meta_in[4:8]

    far = nz // 2
    z_meta, z_inv, z_data = {}, {}, {}

    def send_block(direction, d, h):
        step = 1 if direction == 0 else -1
        src, dst = ((nz - d + 1) % nz, nz - d) if direction == 0 else (d - 1, d)
        part_rows = pl.ds(h * half, half)
        z_data[direction, d, h] = push(
            blocks.at[src, part_rows], blocks.at[dst, part_rows], device(dz=step)
        )

    def send_small(kept, array, direction, d):
        step = 1 if direction == 0 else -1
        src, dst = ((nz - d + 1) % nz, nz - d) if direction == 0 else (d - 1, d)
        kept[direction, d] = push(array.at[src], array.at[dst], device(dz=step))

    token_load.wait()
    pl.semaphore_wait(barrier, len(peers))
    for h in range(2):
        for direction in range(2):
            send_block(direction, 1, h)
    values = blocks[0].astype(F32)
    all_tokens = pl.ds(0, n_tok)
    norm_copies = start_norm(values, 0, all_tokens)
    place()
    for direction in range(2):
        send_small(z_meta, meta, direction, 1)
    inv[0] = end_norm(norm_copies, 0, all_tokens)
    for direction in range(2):
        send_small(z_inv, inv, direction, 1)

    def normalized(r):
        values = blocks[r].astype(F32)
        return (values * spread(inv[r], values.shape[1]) * gain[...]).astype(BF)

    normed[...] = normalized(0)

    x_copies, ret_copies, flight = {}, {}, {}

    def slot_ids(shape):
        s = lax.broadcasted_iota(jnp.int32, shape, 0)
        per = 4 * CAP
        return (z * (NX * per) + (x + s // per) % NX * per + s % per).astype(F32)

    def phase_a(i):
        if i == 0:
            return
        for direction in range(2):
            for kept, array in ((z_meta, meta), (z_inv, inv)):
                if (direction, i) in kept:
                    got(kept[direction, i])
                    if i + 1 < far or (i + 1 == far and direction == 0):
                        send_small(kept, array, direction, i + 1)
        for h in range(2):
            for direction in range(2):
                if (direction, i, h) in z_data:
                    got(z_data[direction, i, h])
                    if i + 1 < far or (i + 1 == far and h == direction):
                        send_block(direction, i + 1, h)

    def phase_b(i):
        for r in STAGES[i]:
            ids = slot_ids((n_tok, n_tok))
            pick = jnp.zeros((n_tok, n_tok), F32)
            for k in range(4):
                pick = jnp.where(ids == meta[r, k : k + 1], 1.0, pick)
            rows = jnp.dot(
                pick.astype(BF),
                normed[...] if r == 0 else normalized(r),
                preferred_element_type=F32,
            ).astype(BF)
            rows = rows.reshape(NX, 4, CAP, rows.shape[-1])
            rows_in[r, 0] = rows[0]
            for dx in range(1, NX):
                rows_out[r, dx] = rows[dx]
            x_copies[r] = [
                push(rows_out.at[r, dx], rows_in.at[r, dx], device(dx=dx)) for dx in range(1, NX)
            ]

    def span(i):
        n = 64 * (1 if i == SHARED else len(STAGES[i]))
        return pl.ds(OFFSET[i], n), n

    def phase_c(i):
        rows, n = span(i)
        need("shared")
        if i != SHARED:
            need("up")
            for r in STAGES[i]:
                for copy in x_copies[r]:
                    got(copy)

        def one(dy, carry):
            e = (y + dy) % ny
            w = 4 if i == SHARED else e
            taken = []
            for core in (1 - c, c):
                if i == SHARED:
                    taken.append(normed[pl.ds(pl.multiple_of((e * 2 + core) * 64, 64), 64)])
                else:
                    for r in STAGES[i]:
                        for k in range(2):
                            taken.append(rows_in[r, core * 2 + k, e])
            left = jnp.concatenate(taken, axis=0)
            for at, weights in ((0, wg), (1, wu)):
                got = jnp.dot(left, weights[w], preferred_element_type=F32).astype(BF)
                cols = pl.ds(at * 512, 512)
                for_partner[dy, rows, cols] = got[:n]
                own_part[dy, rows, cols] = got[n:]
            return carry

        lax.fori_loop(0, ny, one, 0)
        flight["d", i] = push(
            for_partner.at[:, rows], from_partner.at[:, rows], device(dc=1)
        )

    def phase_d(i):
        rows, n = span(i)
        got(flight["d", i])
        flight["y", i] = []
        for dy in range(1, ny):
            own_part[dy, rows] = (
                own_part[dy, rows].astype(F32) + from_partner[dy, rows].astype(F32)
            ).astype(BF)
            flight["y", i].append(
                push(own_part.at[dy, rows], from_y.at[dy - 1, rows], device(dy=dy))
            )

    def phase_e(i):
        rows, n = span(i)
        for copy in flight["y", i]:
            got(copy)
        pre = own_part[0, rows].astype(F32) + from_partner[0, rows].astype(F32)
        for dy in range(1, ny):
            pre = pre + from_y[dy - 1, rows].astype(F32)
        gate, up = pre[:, :512], pre[:, 512:]
        hid[0, 0, rows] = (gate / (1.0 + jnp.exp(-gate)) * up).astype(BF)
        flight["h", i] = [
            push(hid.at[0, 0, rows], hid.at[0, ny - dy, rows], device(dy=dy))
            for dy in range(1, ny)
        ]

    def phase_f(i):
        rows, n = span(i)
        for copy in flight["h", i]:
            got(copy)
        flight["g", i] = push(hid.at[0, :, rows], hid.at[1, :, rows], device(dc=1))

    def phase_g(i):
        rows, n = span(i)
        need("down")
        got(flight["g", i])
        if i != SHARED:
            for r in STAGES[i]:
                sent(x_copies[r])

        def one(dy, carry):
            e = (y + dy) % ny
            w = 4 if i == SHARED else e
            left = jnp.concatenate([hid[0, dy, rows], hid[1, dy, rows]], axis=0)
            got = jnp.dot(left, wd[w], preferred_element_type=F32).astype(BF)
            for at, core in ((0, c), (n, 1 - c)):
                if i == SHARED:
                    shared_out[pl.ds(pl.multiple_of((e * 2 + core) * 64, 64), 64)] = got[
                        at : at + n
                    ]
                else:
                    for j, r in enumerate(STAGES[i]):
                        for k in range(2):
                            first = at + j * 64 + k * CAP
                            rows_out[r, core * 2 + k, e] = got[first : first + CAP]
            return carry

        lax.fori_loop(0, ny, one, 0)
        if i != SHARED:
            for r in STAGES[i]:
                ret_copies[r] = [
                    push(rows_out.at[r, dx], returned.at[r, dx - 1], device(dx=-dx))
                    for dx in range(1, NX)
                ]

    def combine(r):
        for copy in ret_copies[r]:
            got(copy)
        ids = slot_ids((n_tok, n_tok))
        weight = jnp.zeros((n_tok, n_tok), F32)
        for k in range(4):
            weight = jnp.where(ids == meta[r, k : k + 1], meta[r, 4 + k : 5 + k], weight)
        expert_rows = jnp.concatenate(
            [rows_out[r, 0].reshape(4 * CAP, -1), returned[r].reshape(3 * 4 * CAP, -1)], axis=0
        )
        return lax.dot_general(
            weight.astype(BF), expert_rows, (((0,), (0,)), ((), ())), preferred_element_type=F32
        )

    z_sum = {}
    z_slot = {(0, 1): 0, (1, 1): 1, (0, 2): 2, (1, 2): 3, (0, 3): 4, (1, 3): 5, (0, 0): 6, (1, 0): 7}

    def send_sum(direction, r, h):
        d = (r if direction == 0 else nz - r) - 1
        rows = pl.ds(h * half, half)
        z_sum[direction, d, h] = push(
            blocks.at[r, rows], z_in.at[z_slot[direction, d], rows],
            device(dz=1 if direction == 0 else -1),
        )

    def phase_z(d):
        if d == far:
            total = combine(far)
            blocks[far] = total.astype(BF)
            send_sum(0, far, 0)
            send_sum(1, far, 1)
            return
        if d > 0:
            for direction, r in ((0, d), (1, nz - d)):
                part[direction] = combine(r)
            for h in range(2):
                rows = pl.ds(h * half, half)
                for direction, r in ((0, d), (1, nz - d)):
                    total = part[direction, rows]
                    if (direction, d, h) in z_sum:
                        got(z_sum[direction, d, h])
                        total = total + z_in[z_slot[direction, d], rows].astype(F32)
                    for key in [k for k in z_data if source_of(k) == (r, h)]:
                        sent([z_data.pop(key)])
                    blocks[r, rows] = total.astype(BF)
                    send_sum(direction, r, h)
            return
        part[0] = combine(0) + shared_out[...].astype(F32)
        copies = []
        for h in range(2):
            rows = pl.ds(h * half, half)
            total = part[0, rows]
            for direction in range(2):
                got(z_sum[direction, 0, h])
                total = total + z_in[z_slot[direction, 0], rows].astype(F32)
            mix[rows] = total
            copies.append(start_norm(total, 1, rows))
        for h in range(2):
            rows = pl.ds(h * half, half)
            inverse = spread(end_norm(copies[h], 1, rows), mix.shape[1])
            out_ref[rows] = (mix[rows] * inverse * post[...]).astype(BF)

    def source_of(key):
        direction, d, h = key
        return ((nz - d + 1) % nz if direction == 0 else d - 1, h)

    phases = dict(
        A=phase_a, B=phase_b, C=phase_c, D=phase_d, E=phase_e, F=phase_f, G=phase_g, Z=phase_z
    )
    for item in schedule:
        phases[item[0]](int(item[1]))

    sent(list(sends.values()))
    for copy in list(awaited.values()):
        got(copy)
    for name in list(weight_loads):
        need(name)


def per_device(mesh_shape, schedule, tokens, routes, route_weights, pre_gain, eg, eu, ed, sg, su, sd, post_gain):
    n_tok, width = tokens.shape
    nz, ny = mesh_shape["ep"] // NX, mesh_shape["tp"] // NC
    meta = jnp.concatenate([routes.T.astype(F32), route_weights.T], axis=0)
    local = eg.shape[0]
    hidden = eg.shape[2]
    vmem = pl.BlockSpec(memory_space=pltpu.VMEM)
    hbm = pl.BlockSpec(memory_space=pl.ANY)
    nsem = 200
    return pl.pallas_call(
        functools.partial(kernel, nz, ny, width * mesh_shape["tp"], schedule),
        out_shape=jax.ShapeDtypeStruct((n_tok, width), BF),
        in_specs=[hbm, vmem, vmem, vmem] + [hbm] * 6,
        out_specs=vmem,
        scratch_shapes=[
            pltpu.VMEM((n_tok, width), BF),
            pltpu.VMEM((local + 1, width, hidden), BF),
            pltpu.VMEM((local + 1, width, hidden), BF),
            pltpu.VMEM((local + 1, hidden, width), BF),
            pltpu.VMEM((nz, n_tok, width), BF),
            pltpu.VMEM((nz, 8, n_tok), F32),
            pltpu.VMEM((nz, 1, n_tok), F32),
            pltpu.VMEM((nz, NX, local, CAP, width), BF),
            pltpu.VMEM((nz, NX, local, CAP, width), BF),
            pltpu.VMEM((ny, ROWS, 2 * hidden), BF),
            pltpu.VMEM((ny, ROWS, 2 * hidden), BF),
            pltpu.VMEM((ny, ROWS, 2 * hidden), BF),
            pltpu.VMEM((ny - 1, ROWS, 2 * hidden), BF),
            pltpu.VMEM((2, ny, ROWS, hidden), BF),
            pltpu.VMEM((nz, NX - 1, local, CAP, width), BF),
            pltpu.VMEM((n_tok, width), BF),
            pltpu.VMEM((8, n_tok, width), BF),
            pltpu.VMEM((2, n_tok, width), F32),
            pltpu.VMEM((n_tok, width), F32),
            pltpu.VMEM((2, 8, 1, n_tok), F32),
            pltpu.SemaphoreType.DMA((nsem,)),
            pltpu.SemaphoreType.DMA((nsem,)),
            pltpu.SemaphoreType.DMA((8,)),
        ],
        compiler_params=pltpu.CompilerParams(
            collective_id=0, has_side_effects=True, vmem_limit_bytes=66_000_000
        ),
        name="layer",
    )(tokens, meta, pre_gain[None, :], post_gain[None, :], eg, eu, ed, sg, su, sd)


def solution(mesh, schedule=None):
    in_specs = (
        P("ep", "tp"),
        P("ep", None),
        P("ep", None),
        P("tp"),
        P("ep", "tp", None),
        P("ep", "tp", None),
        P("ep", None, "tp"),
        P("tp", None),
        P("tp", None),
        P(None, "tp"),
        P("tp"),
    )
    return jax.shard_map(
        functools.partial(per_device, dict(mesh.shape), tuple(schedule or SCHEDULE)),
        mesh=mesh,
        in_specs=in_specs,
        out_specs=P("ep", "tp"),
        check_vma=False,
    )
```

time: 434 us -> 182 us (0.42)
  Pallas kernels: 0 us -> 178 us
  waiting for transfers between devices: 162 us -> 0 us
  blocking collectives: 132 us -> 0 us
  local copies, waits for them, and re-layouts: 71.3 us -> 1.87 us
  other arithmetic: 20.9 us -> 2.01 us
  starting transfers between devices: 16.3 us -> 0 us
  matrix products: 16 us -> 0 us
  between operations: 13.4 us -> 0.01 us
    pallas_call x0 -> x1, Pallas kernels: none -> 178 us  [per_device(): pl.pallas_call(functools.partial(kernel, nz, ny, width * mesh_shape['tp']...]
    all_to_all x2 -> x0, blocking collectives: 115 us -> none  [the longest x1 104 us: per_device(): lax.all_to_all(outgoing, 'ep', split_axis=0, concat_axis=2, tiled=True)[0]]
    unnamed x5 -> x0, waiting for transfers between devices: 87 us -> none
    all_to_all x2 -> x0, waiting for transfers between devices: 39.7 us -> none  [the longest x1 38.9 us: per_device(): lax.all_to_all(expert_out[None], 'ep', split_axis=2, concat_axis=0, tiled...]
    all_gather x1 -> x0, waiting for transfers between devices: 35.3 us -> none  [activate(): return lax.all_gather(hidden_share, 'tp', axis=1, tiled=True)]
    scatter x1 -> x0, local copies, waits for them, and re-layouts: 21.3 us -> none  [per_device(): jnp.zeros((rows_all, slice_width), jnp.bfloat16).at[positions]]
    all_gather x1 -> x0, blocking collectives: 17.2 us -> none  [activate(): return lax.all_gather(hidden_share, 'tp', axis=1, tiled=True)]
    all_to_all x2 -> x0, starting transfers between devices: 16.2 us -> none  [the longest x1 9.8 us: per_device(): lax.all_to_all(expert_out[None], 'ep', split_axis=2, concat_axis=0, tiled...]
  transfers between devices with their start and end apart: 5 -> 0, of which waited for: 5 -> 0; matrix products, arithmetic and copies ran while one was open for 2% -> 0% of each run, Pallas kernels for 0% -> 0%
where the time goes in v1:
time: 182 us
  Pallas kernels  178 us (98%)
  other arithmetic  2.01 us (1%)
  local copies, waits for them, and re-layouts  1.87 us (1%)
    pallas_call x1, Pallas kernels, per_device(): pl.pallas_call(functools.partial(kernel, nz, ny, width * mesh_shape['tp']...  178 us

profile of v1, /device:TPU:1, one launch (start us, length us, event | category | flops | bytes accessed | tf_op | source)
XLA Modules:
  0.0 181.7 jit_solution(13058281731207362322)
XLA Ops:
  0.0 0.7 convert_bitcast_fusion
  0.7 1.3 pad_maximum_fusion.meta_in
  2.0 177.8 %layer.1 = bf16[512,512]{1,0:T(8,128)(2,1)} custom-call(bf16[512,512]{1,0:T(8,128)(2,1)} %tok_hbm.1, f32[8,512]{1,0:T(8,128)} %pad_maximum_fusion.meta_in, f32[1,512]{1,0:T(1,128)} %bitcast.6, f32[1,512]{1,0:T(1,128)} %bitcast.7, bf16[4,512,512]{2,1,0:T(8,128)(2,1)} %wg_hbm.1, bf16[4,512,512]{2,1,0:T(8,128)(2,1)} %wu_hbm.1, bf16[4,512,512]{2,1,0:T(8,128)(2,1)} %wd_hbm.1, ...), custom_call_target="tpu_custom_call" | custom-call | tf_op jit(solution)/shard_map/layer/pallas_call | solution.py:467
  179.8 1.9 %copy.13 = bf16[512,512]{1,0:T(8,128)(2,1)} copy(bf16[512,512]{1,0:T(8,128)(2,1)} %layer.1) | data formatting | bytes 1048576

commit v2 on v1

--- a/solution.py
+++ b/solution.py
@@ -14,25 +14,30 @@
 NX, NC = 4, 2
 CAP = 32
 
-STAGES = ((0,), (1, 7), (2, 6), (3, 5), (4,), None)
-SHARED = 5
-OFFSET = (0, 64, 192, 320, 448, 512)
-ROWS = 576
+SHARED = 8
+UNIT = 64
+ROWS = UNIT * (SHARED + 1)
 
 SCHEDULE = " ".join(
     (
-        "A0 B0 C5 D5",
-        "A1 B1 E5 C0",
-        "D0 F5 A2 B2",
-        "E0 C1 D1 A3",
-        "B3 F0 G5 G0",
-        "E1 C2 D2 A4",
-        "B4 F1 G1 E2",
-        "C4 D4 F2 C3",
-        "D3 G2 E4 F4",
-        "G4 E3 F3 G3",
-        "Z4 Z3 Z2 Z1",
-        "Z0",
+        "A0 C8 B0 D8",
+        "A1 a1 B7 C0",
+        "A2 B1 D0 E8",
+        "a2 B6 B2 C7",
+        "A3 D7 C6 D6",
+        "a3 B3 C1 C2",
+        "D2 A4 a4 B4",
+        "C3 E6 D3 C4",
+        "B5 D4 E3 E4",
+        "C5 D5 F3 G3",
+        "F4 G4 E5 E2",
+        "F5 D1 G5 F6",
+        "F2 Z4 G2 E1",
+        "E0 G6 Z3 F1",
+        "E7 G1 z3 F7",
+        "G7 F8 Z2 z2",
+        "Z1 G8 F0 G0",
+        "z1 Z0 z0",
     )
 ).split()
 
@@ -43,7 +48,8 @@
     features,
     schedule,
     tok_hbm,
-    meta_in,
+    routes,
+    route_weights,
     gain,
     post,
     wg_hbm,
@@ -71,7 +77,6 @@
     shared_out,
     z_in,
     part,
-    mix,
     sums,
     send_sem,
     recv_sem,
@@ -181,7 +186,7 @@
         e_id = lax.broadcasted_iota(jnp.int32, (experts, n_tok), 0).astype(F32)
         named = jnp.zeros((experts, n_tok), F32)
         for k in range(4):
-            named += (e_id == meta_in[k : k + 1]).astype(F32)
+            named += (e_id == routes[k : k + 1].astype(F32)).astype(F32)
         before = (
             lax.broadcasted_iota(jnp.int32, (n_tok, n_tok), 0)
             < lax.broadcasted_iota(jnp.int32, (n_tok, n_tok), 1)
@@ -190,10 +195,10 @@
             named.astype(BF), before.astype(F32).astype(BF), preferred_element_type=F32
         )
         for k in range(4):
-            route = meta_in[k : k + 1]
+            route = routes[k : k + 1].astype(F32)
             slot = jnp.sum(jnp.where(e_id == route, counts, 0.0), axis=0, keepdims=True)
             meta[0, k : k + 1] = route * CAP + slot
-        meta[0, 4:8] = meta_in[4:8]
+        meta[0, 4:8] = route_weights[...]
 
     far = nz // 2
     z_meta, z_inv, z_data = {}, {}, {}
@@ -239,53 +244,47 @@
         per = 4 * CAP
         return (z * (NX * per) + (x + s // per) % NX * per + s % per).astype(F32)
 
-    def phase_a(i):
-        if i == 0:
+    def phase_a(d, h):
+        if d == 0:
             return
+        if h == 0:
+            for direction in range(2):
+                for kept, array in ((z_meta, meta), (z_inv, inv)):
+                    if (direction, d) in kept:
+                        got(kept[direction, d])
+                        if d + 1 < far or (d + 1 == far and direction == 0):
+                            send_small(kept, array, direction, d + 1)
         for direction in range(2):
-            for kept, array in ((z_meta, meta), (z_inv, inv)):
-                if (direction, i) in kept:
-                    got(kept[direction, i])
-                    if i + 1 < far or (i + 1 == far and direction == 0):
-                        send_small(kept, array, direction, i + 1)
-        for h in range(2):
-            for direction in range(2):
-                if (direction, i, h) in z_data:
-                    got(z_data[direction, i, h])
-                    if i + 1 < far or (i + 1 == far and h == direction):
-                        send_block(direction, i + 1, h)
-
-    def phase_b(i):
-        for r in STAGES[i]:
-            ids = slot_ids((n_tok, n_tok))
-            pick = jnp.zeros((n_tok, n_tok), F32)
-            for k in range(4):
-                pick = jnp.where(ids == meta[r, k : k + 1], 1.0, pick)
-            rows = jnp.dot(
-                pick.astype(BF),
-                normed[...] if r == 0 else normalized(r),
-                preferred_element_type=F32,
-            ).astype(BF)
-            rows = rows.reshape(NX, 4, CAP, rows.shape[-1])
-            rows_in[r, 0] = rows[0]
-            for dx in range(1, NX):
-                rows_out[r, dx] = rows[dx]
-            x_copies[r] = [
-                push(rows_out.at[r, dx], rows_in.at[r, dx], device(dx=dx)) for dx in range(1, NX)
-            ]
-
-    def span(i):
-        n = 64 * (1 if i == SHARED else len(STAGES[i]))
-        return pl.ds(OFFSET[i], n), n
+            if (direction, d, h) in z_data:
+                got(z_data[direction, d, h])
+                if d + 1 < far or (d + 1 == far and h == direction):
+                    send_block(direction, d + 1, h)
+
+    def phase_b(r):
+        ids = slot_ids((n_tok, n_tok))
+        pick = jnp.zeros((n_tok, n_tok), F32)
+        for k in range(4):
+            pick = jnp.where(ids == meta[r, k : k + 1], 1.0, pick)
+        rows = jnp.dot(
+            pick.astype(BF),
+            normed[...] if r == 0 else normalized(r),
+            preferred_element_type=F32,
+        ).astype(BF)
+        rows = rows.reshape(NX, 4, CAP, rows.shape[-1])
+        rows_in[r, 0] = rows[0]
+        for dx in range(1, NX):
+            rows_out[r, dx] = rows[dx]
+        x_copies[r] = [
+            push(rows_out.at[r, dx], rows_in.at[r, dx], device(dx=dx)) for dx in range(1, NX)
+        ]
 
     def phase_c(i):
-        rows, n = span(i)
+        rows = pl.ds(UNIT * i, UNIT)
         need("shared")
         if i != SHARED:
             need("up")
-            for r in STAGES[i]:
-                for copy in x_copies[r]:
-                    got(copy)
+            for copy in x_copies[i]:
+                got(copy)
 
         def one(dy, carry):
             e = (y + dy) % ny
@@ -293,17 +292,16 @@
             taken = []
             for core in (1 - c, c):
                 if i == SHARED:
-                    taken.append(normed[pl.ds(pl.multiple_of((e * 2 + core) * 64, 64), 64)])
+                    first = pl.multiple_of((e * 2 + core) * UNIT, UNIT)
+                    taken.append(normed[pl.ds(first, UNIT)])
                 else:
-                    for r in STAGES[i]:
-                        for k in range(2):
-                            taken.append(rows_in[r, core * 2 + k, e])
+                    taken += [rows_in[i, core * 2 + k, e] for k in range(2)]
             left = jnp.concatenate(taken, axis=0)
             for at, weights in ((0, wg), (1, wu)):
-                got = jnp.dot(left, weights[w], preferred_element_type=F32).astype(BF)
+                got_rows = jnp.dot(left, weights[w], preferred_element_type=F32).astype(BF)
                 cols = pl.ds(at * 512, 512)
-                for_partner[dy, rows, cols] = got[:n]
-                own_part[dy, rows, cols] = got[n:]
+                for_partner[dy, rows, cols] = got_rows[:UNIT]
+                own_part[dy, rows, cols] = got_rows[UNIT:]
             return carry
 
         lax.fori_loop(0, ny, one, 0)
@@ -312,7 +310,7 @@
         )
 
     def phase_d(i):
-        rows, n = span(i)
+        rows = pl.ds(UNIT * i, UNIT)
         got(flight["d", i])
         flight["y", i] = []
         for dy in range(1, ny):
@@ -324,7 +322,7 @@
             )
 
     def phase_e(i):
-        rows, n = span(i)
+        rows = pl.ds(UNIT * i, UNIT)
         for copy in flight["y", i]:
             got(copy)
         pre = own_part[0, rows].astype(F32) + from_partner[0, rows].astype(F32)
@@ -338,43 +336,39 @@
         ]
 
     def phase_f(i):
-        rows, n = span(i)
+        rows = pl.ds(UNIT * i, UNIT)
         for copy in flight["h", i]:
             got(copy)
         flight["g", i] = push(hid.at[0, :, rows], hid.at[1, :, rows], device(dc=1))
 
     def phase_g(i):
-        rows, n = span(i)
+        rows = pl.ds(UNIT * i, UNIT)
         need("down")
         got(flight["g", i])
         if i != SHARED:
-            for r in STAGES[i]:
-                sent(x_copies[r])
+            sent(x_copies[i])
 
         def one(dy, carry):
             e = (y + dy) % ny
             w = 4 if i == SHARED else e
             left = jnp.concatenate([hid[0, dy, rows], hid[1, dy, rows]], axis=0)
-            got = jnp.dot(left, wd[w], preferred_element_type=F32).astype(BF)
-            for at, core in ((0, c), (n, 1 - c)):
+            out = jnp.dot(left, wd[w], preferred_element_type=F32).astype(BF)
+            for at, core in ((0, c), (UNIT, 1 - c)):
                 if i == SHARED:
-                    shared_out[pl.ds(pl.multiple_of((e * 2 + core) * 64, 64), 64)] = got[
-                        at : at + n
-                    ]
+                    first = pl.multiple_of((e * 2 + core) * UNIT, UNIT)
+                    shared_out[pl.ds(first, UNIT)] = out[at : at + UNIT]
                 else:
-                    for j, r in enumerate(STAGES[i]):
-                        for k in range(2):
-                            first = at + j * 64 + k * CAP
-                            rows_out[r, core * 2 + k, e] = got[first : first + CAP]
+                    for k in range(2):
+                        first = at + k * CAP
+                        rows_out[i, core * 2 + k, e] = out[first : first + CAP]
             return carry
 
         lax.fori_loop(0, ny, one, 0)
         if i != SHARED:
-            for r in STAGES[i]:
-                ret_copies[r] = [
-                    push(rows_out.at[r, dx], returned.at[r, dx - 1], device(dx=-dx))
-                    for dx in range(1, NX)
-                ]
+            ret_copies[i] = [
+                push(rows_out.at[i, dx], returned.at[i, dx - 1], device(dx=-dx))
+                for dx in range(1, NX)
+            ]
 
     def combine(r):
         for copy in ret_copies[r]:
@@ -401,52 +395,58 @@
             device(dz=1 if direction == 0 else -1),
         )
 
-    def phase_z(d):
+    def ways(d):
+        return ((0, d, 2 * (d % 2)), (1, (nz - d) % nz, 2 * (d % 2) + 1))
+
+    def phase_z(d, h):
+        rows = pl.ds(h * half, half)
         if d == far:
             total = combine(far)
             blocks[far] = total.astype(BF)
             send_sum(0, far, 0)
             send_sum(1, far, 1)
             return
+        if h == 0:
+            if d > 0:
+                for direction, r, slot in ways(d):
+                    part[slot] = combine(r)
+            else:
+                part[0] = combine(0) + shared_out[...].astype(F32)
         if d > 0:
-            for direction, r in ((0, d), (1, nz - d)):
-                part[direction] = combine(r)
-            for h in range(2):
-                rows = pl.ds(h * half, half)
-                for direction, r in ((0, d), (1, nz - d)):
-                    total = part[direction, rows]
-                    if (direction, d, h) in z_sum:
-                        got(z_sum[direction, d, h])
-                        total = total + z_in[z_slot[direction, d], rows].astype(F32)
-                    for key in [k for k in z_data if source_of(k) == (r, h)]:
-                        sent([z_data.pop(key)])
-                    blocks[r, rows] = total.astype(BF)
-                    send_sum(direction, r, h)
+            for direction, r, slot in ways(d):
+                total = part[slot, rows]
+                if (direction, d, h) in z_sum:
+                    got(z_sum[direction, d, h])
+                    total = total + z_in[z_slot[direction, d], rows].astype(F32)
+                for key in [k for k in z_data if source_of(k) == (r, h)]:
+                    sent([z_data.pop(key)])
+                blocks[r, rows] = total.astype(BF)
+                send_sum(direction, r, h)
             return
-        part[0] = combine(0) + shared_out[...].astype(F32)
-        copies = []
-        for h in range(2):
-            rows = pl.ds(h * half, half)
-            total = part[0, rows]
-            for direction in range(2):
-                got(z_sum[direction, 0, h])
-                total = total + z_in[z_slot[direction, 0], rows].astype(F32)
-            mix[rows] = total
-            copies.append(start_norm(total, 1, rows))
-        for h in range(2):
-            rows = pl.ds(h * half, half)
-            inverse = spread(end_norm(copies[h], 1, rows), mix.shape[1])
-            out_ref[rows] = (mix[rows] * inverse * post[...]).astype(BF)
+        total = part[0, rows]
+        for direction in range(2):
+            got(z_sum[direction, 0, h])
+            total = total + z_in[z_slot[direction, 0], rows].astype(F32)
+        part[0, rows] = total
+        flight["n", h] = start_norm(total, 1, rows)
+        if h == 1:
+            for k in range(2):
+                rows = pl.ds(k * half, half)
+                inverse = spread(end_norm(flight["n", k], 1, rows), part.shape[2])
+                out_ref[rows] = (part[0, rows] * inverse * post[...]).astype(BF)
 
     def source_of(key):
         direction, d, h = key
         return ((nz - d + 1) % nz if direction == 0 else d - 1, h)
 
-    phases = dict(
-        A=phase_a, B=phase_b, C=phase_c, D=phase_d, E=phase_e, F=phase_f, G=phase_g, Z=phase_z
-    )
+    phases = dict(B=phase_b, C=phase_c, D=phase_d, E=phase_e, F=phase_f, G=phase_g)
+    halves = dict(A=(phase_a, 0), a=(phase_a, 1), Z=(phase_z, 0), z=(phase_z, 1))
     for item in schedule:
-        phases[item[0]](int(item[1]))
+        if item[0] in phases:
+            phases[item[0]](int(item[1]))
+        else:
+            phase, h = halves[item[0]]
+            phase(int(item[1]), h)
 
     sent(list(sends.values()))
     for copy in list(awaited.values()):
@@ -458,16 +458,15 @@
 def per_device(mesh_shape, schedule, tokens, routes, route_weights, pre_gain, eg, eu, ed, sg, su, sd, post_gain):
     n_tok, width = tokens.shape
     nz, ny = mesh_shape["ep"] // NX, mesh_shape["tp"] // NC
-    meta = jnp.concatenate([routes.T.astype(F32), route_weights.T], axis=0)
     local = eg.shape[0]
     hidden = eg.shape[2]
     vmem = pl.BlockSpec(memory_space=pltpu.VMEM)
     hbm = pl.BlockSpec(memory_space=pl.ANY)
-    nsem = 200
+    nsem = 240
     return pl.pallas_call(
         functools.partial(kernel, nz, ny, width * mesh_shape["tp"], schedule),
         out_shape=jax.ShapeDtypeStruct((n_tok, width), BF),
-        in_specs=[hbm, vmem, vmem, vmem] + [hbm] * 6,
+        in_specs=[hbm] + [vmem] * 4 + [hbm] * 6,
         out_specs=vmem,
         scratch_shapes=[
             pltpu.VMEM((n_tok, width), BF),
@@ -487,8 +486,7 @@
             pltpu.VMEM((nz, NX - 1, local, CAP, width), BF),
             pltpu.VMEM((n_tok, width), BF),
             pltpu.VMEM((8, n_tok, width), BF),
-            pltpu.VMEM((2, n_tok, width), F32),
-            pltpu.VMEM((n_tok, width), F32),
+            pltpu.VMEM((4, n_tok, width), F32),
             pltpu.VMEM((2, 8, 1, n_tok), F32),
             pltpu.SemaphoreType.DMA((nsem,)),
             pltpu.SemaphoreType.DMA((nsem,)),
@@ -498,7 +496,19 @@
             collective_id=0, has_side_effects=True, vmem_limit_bytes=66_000_000
         ),
         name="layer",
-    )(tokens, meta, pre_gain[None, :], post_gain[None, :], eg, eu, ed, sg, su, sd)
+    )(
+        tokens,
+        routes.T,
+        route_weights.T,
+        pre_gain[None, :],
+        post_gain[None, :],
+        eg,
+        eu,
+        ed,
+        sg,
+        su,
+        sd,
+    )
 
 
 def solution(mesh, schedule=None):

time: 182 us -> 155 us (0.85)
  Pallas kernels: 178 us -> 153 us
  other arithmetic: 2.01 us -> 0 us
    pallas_call x1, Pallas kernels: 178 us -> 153 us  [per_device(): pl.pallas_call(functools.partial(kernel, nz, ny, width * mesh_shape['tp']...]
where the time goes in v2:
time: 155 us
  Pallas kernels  153 us (99%)
  local copies, waits for them, and re-layouts  1.87 us (1%)
    pallas_call x1, Pallas kernels, per_device(): pl.pallas_call(functools.partial(kernel, nz, ny, width * mesh_shape['tp']...  153 us

profile of v2, /device:TPU:1, one launch (start us, length us, event | category | flops | bytes accessed | tf_op | source)
XLA Modules:
  0.0 155.2 jit_solution(10611518322075700652)
XLA Ops:
  0.0 153.3 %layer.1 = bf16[512,512]{1,0:T(8,128)(2,1)} custom-call(bf16[512,512]{1,0:T(8,128)(2,1)} %tok_hbm.1, s32[4,512]{1,0:T(4,128)} %bitcast.4, f32[4,512]{1,0:T(4,128)} %bitcast.5, f32[1,512]{1,0:T(1,128)} %bitcast.6, f32[1,512]{1,0:T(1,128)} %bitcast.7, bf16[4,512,512]{2,1,0:T(8,128)(2,1)} %wg_hbm.1, bf16[4,512,512]{2,1,0:T(8,128)(2,1)} %wu_hbm.1, ...), custom_call_target="tpu_custom_call" | custom-call | tf_op jit(solution)/shard_map/layer/pallas_call | solution.py:466
  153.3 1.9 %copy.13 = bf16[512,512]{1,0:T(8,128)(2,1)} copy(bf16[512,512]{1,0:T(8,128)(2,1)} %layer.1) | data formatting | bytes 1048576

commit v3 on v2

--- a/solution.py
+++ b/solution.py
@@ -27,9 +27,9 @@
         "A3 D7 C6 D6",
         "a3 B3 C1 C2",
         "D2 A4 a4 B4",
-        "C3 E6 D3 C4",
-        "B5 D4 E3 E4",
-        "C5 D5 F3 G3",
+        "C3 D3 C4 B5",
+        "D4 E3 E4 C5",
+        "D5 E6 F3 G3",
         "F4 G4 E5 E2",
         "F5 D1 G5 F6",
         "F2 Z4 G2 E1",
@@ -51,7 +51,6 @@
     routes,
     route_weights,
     gain,
-    post,
     wg_hbm,
     wu_hbm,
     wd_hbm,
@@ -94,6 +93,9 @@
             (y + dy + ny) % ny * NC + (c + dc) % NC,
         )
 
+    def far_first(n):
+        return sorted(range(1, n), key=lambda k: -min(k, n - k))
+
     used = [0, 0]
     sends, awaited = {}, {}
 
@@ -218,9 +220,8 @@
 
     token_load.wait()
     pl.semaphore_wait(barrier, len(peers))
-    for h in range(2):
-        for direction in range(2):
-            send_block(direction, 1, h)
+    for direction, h in ((0, 0), (1, 1), (0, 1), (1, 0)):
+        send_block(direction, 1, h)
     values = blocks[0].astype(F32)
     all_tokens = pl.ds(0, n_tok)
     norm_copies = start_norm(values, 0, all_tokens)
@@ -244,10 +245,10 @@
         per = 4 * CAP
         return (z * (NX * per) + (x + s // per) % NX * per + s % per).astype(F32)
 
-    def phase_a(d, h):
+    def phase_a(d, second):
         if d == 0:
             return
-        if h == 0:
+        if second == 0:
             for direction in range(2):
                 for kept, array in ((z_meta, meta), (z_inv, inv)):
                     if (direction, d) in kept:
@@ -255,6 +256,7 @@
                         if d + 1 < far or (d + 1 == far and direction == 0):
                             send_small(kept, array, direction, d + 1)
         for direction in range(2):
+            h = direction if second == 0 else 1 - direction
             if (direction, d, h) in z_data:
                 got(z_data[direction, d, h])
                 if d + 1 < far or (d + 1 == far and h == direction):
@@ -275,7 +277,7 @@
         for dx in range(1, NX):
             rows_out[r, dx] = rows[dx]
         x_copies[r] = [
-            push(rows_out.at[r, dx], rows_in.at[r, dx], device(dx=dx)) for dx in range(1, NX)
+            push(rows_out.at[r, dx], rows_in.at[r, dx], device(dx=dx)) for dx in far_first(NX)
         ]
 
     def phase_c(i):
@@ -304,7 +306,7 @@
                 own_part[dy, rows, cols] = got_rows[UNIT:]
             return carry
 
-        lax.fori_loop(0, ny, one, 0)
+        lax.fori_loop(0, ny, one, 0, unroll=True)
         flight["d", i] = push(
             for_partner.at[:, rows], from_partner.at[:, rows], device(dc=1)
         )
@@ -313,7 +315,7 @@
         rows = pl.ds(UNIT * i, UNIT)
         got(flight["d", i])
         flight["y", i] = []
-        for dy in range(1, ny):
+        for dy in far_first(ny):
             own_part[dy, rows] = (
                 own_part[dy, rows].astype(F32) + from_partner[dy, rows].astype(F32)
             ).astype(BF)
@@ -332,7 +334,7 @@
         hid[0, 0, rows] = (gate / (1.0 + jnp.exp(-gate)) * up).astype(BF)
         flight["h", i] = [
             push(hid.at[0, 0, rows], hid.at[0, ny - dy, rows], device(dy=dy))
-            for dy in range(1, ny)
+            for dy in far_first(ny)
         ]
 
     def phase_f(i):
@@ -363,11 +365,11 @@
                         rows_out[i, core * 2 + k, e] = out[first : first + CAP]
             return carry
 
-        lax.fori_loop(0, ny, one, 0)
+        lax.fori_loop(0, ny, one, 0, unroll=True)
         if i != SHARED:
             ret_copies[i] = [
                 push(rows_out.at[i, dx], returned.at[i, dx - 1], device(dx=-dx))
-                for dx in range(1, NX)
+                for dx in far_first(NX)
             ]
 
     def combine(r):
@@ -398,15 +400,14 @@
     def ways(d):
         return ((0, d, 2 * (d % 2)), (1, (nz - d) % nz, 2 * (d % 2) + 1))
 
-    def phase_z(d, h):
-        rows = pl.ds(h * half, half)
+    def phase_z(d, second):
         if d == far:
             total = combine(far)
             blocks[far] = total.astype(BF)
             send_sum(0, far, 0)
             send_sum(1, far, 1)
             return
-        if h == 0:
+        if second == 0:
             if d > 0:
                 for direction, r, slot in ways(d):
                     part[slot] = combine(r)
@@ -414,6 +415,8 @@
                 part[0] = combine(0) + shared_out[...].astype(F32)
         if d > 0:
             for direction, r, slot in ways(d):
+                h = second if direction == 1 else 1 - second
+                rows = pl.ds(h * half, half)
                 total = part[slot, rows]
                 if (direction, d, h) in z_sum:
                     got(z_sum[direction, d, h])
@@ -423,17 +426,24 @@
                 blocks[r, rows] = total.astype(BF)
                 send_sum(direction, r, h)
             return
-        total = part[0, rows]
-        for direction in range(2):
-            got(z_sum[direction, 0, h])
-            total = total + z_in[z_slot[direction, 0], rows].astype(F32)
-        part[0, rows] = total
-        flight["n", h] = start_norm(total, 1, rows)
-        if h == 1:
-            for k in range(2):
-                rows = pl.ds(k * half, half)
-                inverse = spread(end_norm(flight["n", k], 1, rows), part.shape[2])
-                out_ref[rows] = (part[0, rows] * inverse * post[...]).astype(BF)
+        if second == 0:
+            return
+        for h in range(2):
+            rows = pl.ds(h * half, half)
+            total = part[0, rows]
+            for direction in (1 - h, h):
+                got(z_sum[direction, 0, h])
+                total = total + z_in[z_slot[direction, 0], rows].astype(F32)
+            part[0, rows] = total
+            flight["n", h] = start_norm(total, 1, rows)
+        for h in range(2):
+            finish(h)
+
+    def finish(h):
+        rows = pl.ds(h * half, half)
+        inverse = spread(end_norm(flight["n", h], 1, rows), part.shape[2])
+        part[1, rows] = part[0, rows] * inverse
+        flight["out", h] = load(part.at[1, rows], out_ref.at[rows])
 
     def source_of(key):
         direction, d, h = key
@@ -449,6 +459,9 @@
             phase(int(item[1]), h)
 
     sent(list(sends.values()))
+    for h in range(2):
+        if ("out", h) in flight:
+            flight["out", h].wait()
     for copy in list(awaited.values()):
         got(copy)
     for name in list(weight_loads):
@@ -463,11 +476,11 @@
     vmem = pl.BlockSpec(memory_space=pltpu.VMEM)
     hbm = pl.BlockSpec(memory_space=pl.ANY)
     nsem = 240
-    return pl.pallas_call(
+    scaled = pl.pallas_call(
         functools.partial(kernel, nz, ny, width * mesh_shape["tp"], schedule),
-        out_shape=jax.ShapeDtypeStruct((n_tok, width), BF),
-        in_specs=[hbm] + [vmem] * 4 + [hbm] * 6,
-        out_specs=vmem,
+        out_shape=jax.ShapeDtypeStruct((n_tok, width), F32),
+        in_specs=[hbm] + [vmem] * 3 + [hbm] * 6,
+        out_specs=hbm,
         scratch_shapes=[
             pltpu.VMEM((n_tok, width), BF),
             pltpu.VMEM((local + 1, width, hidden), BF),
@@ -490,7 +503,7 @@
             pltpu.VMEM((2, 8, 1, n_tok), F32),
             pltpu.SemaphoreType.DMA((nsem,)),
             pltpu.SemaphoreType.DMA((nsem,)),
-            pltpu.SemaphoreType.DMA((8,)),
+            pltpu.SemaphoreType.DMA((12,)),
         ],
         compiler_params=pltpu.CompilerParams(
             collective_id=0, has_side_effects=True, vmem_limit_bytes=66_000_000
@@ -501,7 +514,6 @@
         routes.T,
         route_weights.T,
         pre_gain[None, :],
-        post_gain[None, :],
         eg,
         eu,
         ed,
@@ -509,6 +521,7 @@
         su,
         sd,
     )
+    return (scaled * post_gain[None, :]).astype(BF)
 
 
 def solution(mesh, schedule=None):

time: 155 us -> 153 us (0.987)
  Pallas kernels: 153 us -> 150 us
  other arithmetic: 0 us -> 2.14 us
  local copies, waits for them, and re-layouts: 1.87 us -> 0.01 us
    pallas_call x1, Pallas kernels: 153 us -> 150 us  [per_device(): pl.pallas_call(functools.partial(kernel, nz, ny, width * mesh_shape['tp']...]
    convert_element_type x0 -> x1, other arithmetic: none -> 2.14 us  [per_device(): return (scaled * post_gain[None, :]).astype(BF)]
    unnamed x1 -> x2, local copies, waits for them, and re-layouts: 1.87 us -> 0.01 us
where the time goes in v3:
time: 153 us; the launch traced here: 152 us
  Pallas kernels  150 us (98%)
  other arithmetic  2.14 us (1%)
    pallas_call x1, Pallas kernels, per_device(): pl.pallas_call(functools.partial(kernel, nz, ny, width * mesh_shape['tp']...  150 us

profile of v3, /device:TPU:1, one launch (start us, length us, event | category | flops | bytes accessed | tf_op | source)
XLA Modules:
  0.0 152.4 jit_solution(836977117696653535)
XLA Ops:
  0.0 0.0 copy-start
  0.0 150.2 %layer.1 = f32[512,512]{1,0:T(8,128)} custom-call(bf16[512,512]{1,0:T(8,128)(2,1)} %tok_hbm.1, s32[4,512]{1,0:T(4,128)} %bitcast.3, f32[4,512]{1,0:T(4,128)} %bitcast.4, f32[1,512]{1,0:T(1,128)} %bitcast.5, bf16[4,512,512]{2,1,0:T(8,128)(2,1)} %wg_hbm.1, bf16[4,512,512]{2,1,0:T(8,128)(2,1)} %wu_hbm.1, bf16[4,512,512]{2,1,0:T(8,128)(2,1)} %wd_hbm.1, ...), custom_call_target="tpu_custom_call" | custom-call | tf_op jit(solution)/shard_map/layer/pallas_call | solution.py:479
  150.2 0.0 copy-done
  150.2 2.1 %multiply_convert_fusion = bf16[512,512]{1,0:T(8,128)(2,1)} fusion(f32[512,512]{1,0:T(8,128)} %layer.1, f32[512]{0:T(512)S(1)} %copy-done), kind=kLoop, calls=%fused_computation | loop fusion | flops 524288 | bytes 1574912 | tf_op jit(solution)/shard_map/convert_element_type | solution.py:524
Async XLA Ops:
  0.0 150.2 %copy-start = (f32[512]{0:T(512)S(1)}, f32[512]{0:T(512)}, u32[]{:S(2)}) copy-start(f32[512]{0:T(512)} %param.21) | copy-start | bytes 6148

commit v4 on v3

--- a/solution.py
+++ b/solution.py
@@ -427,13 +427,16 @@
                 send_sum(direction, r, h)
             return
         if second == 0:
+            for direction in range(2):
+                h = 1 - direction
+                rows = pl.ds(h * half, half)
+                got(z_sum[direction, 0, h])
+                part[0, rows] = part[0, rows] + z_in[z_slot[direction, 0], rows].astype(F32)
             return
         for h in range(2):
             rows = pl.ds(h * half, half)
-            total = part[0, rows]
-            for direction in (1 - h, h):
-                got(z_sum[direction, 0, h])
-                total = total + z_in[z_slot[direction, 0], rows].astype(F32)
+            got(z_sum[h, 0, h])
+            total = part[0, rows] + z_in[z_slot[h, 0], rows].astype(F32)
             part[0, rows] = total
             flight["n", h] = start_norm(total, 1, rows)
         for h in range(2):

time: 153 us -> 152 us (level)
  no operation moved by 1% of the time
where the time goes in v4:
time: 152 us
  Pallas kernels  150 us (99%)
  other arithmetic  2.14 us (1%)
    pallas_call x1, Pallas kernels, per_device(): pl.pallas_call(functools.partial(kernel, nz, ny, width * mesh_shape['tp']...  150 us

profile of v4, /device:TPU:1, one launch (start us, length us, event | category | flops | bytes accessed | tf_op | source)
XLA Modules:
  0.0 152.3 jit_solution(307079354046297785)
XLA Ops:
  0.0 0.0 copy-start
  0.0 150.2 %layer.1 = f32[512,512]{1,0:T(8,128)} custom-call(bf16[512,512]{1,0:T(8,128)(2,1)} %tok_hbm.1, s32[4,512]{1,0:T(4,128)} %bitcast.3, f32[4,512]{1,0:T(4,128)} %bitcast.4, f32[1,512]{1,0:T(1,128)} %bitcast.5, bf16[4,512,512]{2,1,0:T(8,128)(2,1)} %wg_hbm.1, bf16[4,512,512]{2,1,0:T(8,128)(2,1)} %wu_hbm.1, bf16[4,512,512]{2,1,0:T(8,128)(2,1)} %wd_hbm.1, ...), custom_call_target="tpu_custom_call" | custom-call | tf_op jit(solution)/shard_map/layer/pallas_call | solution.py:482
  150.2 0.0 copy-done
  150.2 2.1 %multiply_convert_fusion = bf16[512,512]{1,0:T(8,128)(2,1)} fusion(f32[512,512]{1,0:T(8,128)} %layer.1, f32[512]{0:T(512)S(1)} %copy-done), kind=kLoop, calls=%fused_computation | loop fusion | flops 524288 | bytes 1574912 | tf_op jit(solution)/shard_map/convert_element_type | solution.py:527
Async XLA Ops:
  0.0 150.2 %copy-start = (f32[512]{0:T(512)S(1)}, f32[512]{0:T(512)}, u32[]{:S(2)}) copy-start(f32[512]{0:T(512)} %param.21) | copy-start | bytes 6148
